TPU v7x, 32 devices: a whole 2x2x4 slice. The times are simulated.
32 devices in a mesh: fs: 4 (over y, x), tp: 8 (over z, core).
Axes of the slice: x: 2, y: 2, z: 4, core: 2. Of those that a mesh axis runs over, the one named last changes fastest.
Arguments:
- normed_inputs: bfloat16 [4096, 4096], P('fs', 'tp'), may hold values from -6 to 6
- query_upstream: bfloat16 [4096, 4096], P('fs', 'tp'), may hold values from -0.125 to 0.125
- key_upstream: bfloat16 [4096, 1024], P('fs', 'tp'), may hold values from -0.09375 to 0.09375
- head_outputs: bfloat16 [4096, 4096], P('fs', 'tp'), may hold values from -6 to 6
- branch_upstream: bfloat16 [4096, 4096], P('fs', 'tp'), may hold values from -0.125 to 0.125
- query_master: float32 [4096, 4096], P('fs', 'tp'), may hold values from -0.09375 to 0.09375
- key_master: float32 [4096, 1024], P('fs', 'tp'), may hold values from -0.09375 to 0.09375
- branch_master: float32 [4096, 4096], P('fs', 'tp'), may hold values from -0.09375 to 0.09375
- query_basis: bfloat16 [4096, 128], replicated, may hold values from -0.09375 to 0.09375
- key_basis: bfloat16 [4096, 128], replicated, may hold values from -0.09375 to 0.09375
- branch_basis: bfloat16 [4096, 128], replicated, may hold values from -0.09375 to 0.09375
- query_first: float32 [128, 4096], P(None, 'tp'), may hold values from -0.75 to 0.75
- query_second: float32 [128, 4096], P(None, 'tp'), may hold values from 0.001 to 0.02
- key_first: float32 [128, 1024], P(None, 'tp'), may hold values from -0.75 to 0.75
- key_second: float32 [128, 1024], P(None, 'tp'), may hold values from 0.001 to 0.02
- branch_first: float32 [4096, 128], P('fs'), may hold values from -0.75 to 0.75
- branch_second: float32 [4096, 128], P('fs'), may hold values from 0.001 to 0.02
Outputs:
- query_step: float32 [4096, 4096], P('fs', 'tp')
- key_step: float32 [4096, 1024], P('fs', 'tp')
- branch_step: float32 [4096, 4096], P('fs', 'tp')
- query_updated: float32 [4096, 4096], P('fs', 'tp')
- key_updated: float32 [4096, 1024], P('fs', 'tp')
- branch_updated: float32 [4096, 4096], P('fs', 'tp')
- query_copy: bfloat16 [4096, 4096], P(None, 'tp')
- key_copy: bfloat16 [4096, 1024], P(None, 'tp')
- branch_copy: bfloat16 [4096, 4096], P(None, 'tp')
- query_first_new: float32 [128, 4096], P(None, 'tp')
- query_second_new: float32 [128, 4096], P(None, 'tp')
- key_first_new: float32 [128, 1024], P(None, 'tp')
- key_second_new: float32 [128, 1024], P(None, 'tp')
- branch_first_new: float32 [4096, 128], P('fs')
- branch_second_new: float32 [4096, 128], P('fs')
All inputs are finite; a program needn't handle non-finite values.
Results may differ from a plain program's by a relative error of at most 0.001.
Values may be sent and summed in bfloat16 or wider, within the bound.
No kernel may reach another device: no remote copies, remote signals or barrier semaphores. Data moves between devices by JAX's collectives and lax.ppermute only.
A program may use at most 128 MiB of HBM per device.

v0:
```python
import jax
import jax.numpy as jnp
from jax import lax
from jax.sharding import PartitionSpec as P

LEARN = 0.02
BETA_ONE = 0.9
BETA_TWO = 0.95
ADAM_EPS = 1e-08
CLIP_RMS = 0.5


def moments(first, second, low, clip):
    scaled = clip * low
    first_new = BETA_ONE * first + (1.0 - BETA_ONE) * scaled
    second_new = BETA_TWO * second + (1.0 - BETA_TWO) * scaled * scaled
    return (first_new, second_new, first_new / (jnp.sqrt(second_new) + ADAM_EPS))


def over_tokens(left, right, precision=None):
    return lax.dot_general(
        left,
        right,
        (((0,), (0,)), ((), ())),
        precision=precision,
        preferred_element_type=jnp.float32,
    )


def per_device(
    normed_inputs,
    query_upstream,
    key_upstream,
    head_outputs,
    branch_upstream,
    query_master,
    key_master,
    branch_master,
    query_basis,
    key_basis,
    branch_basis,
    query_first,
    query_second,
    key_first,
    key_second,
    branch_first,
    branch_second,
):
    exact = lax.Precision.HIGHEST
    row_index = lax.axis_index("fs")
    col_index = lax.axis_index("tp")
    n_rows = lax.axis_size("fs")
    n_cols = lax.axis_size("tp")
    features = normed_inputs.shape[1]
    query_local = query_upstream.shape[1]
    key_local = key_upstream.shape[1]
    rows_in = query_master.shape[0]
    rank = query_basis.shape[1]
    whole_values = lax.all_gather(head_outputs, "tp", axis=1, tiled=True)
    block_query = lax.dynamic_slice_in_dim(query_basis, col_index * features, features, 0)
    block_key = lax.dynamic_slice_in_dim(key_basis, col_index * features, features, 0)
    proj_query, proj_key = lax.psum(
        (
            jnp.dot(normed_inputs, block_query, preferred_element_type=jnp.float32),
            jnp.dot(normed_inputs, block_key, preferred_element_type=jnp.float32),
        ),
        "tp",
    )
    part_query = over_tokens(proj_query, query_upstream.astype(jnp.float32), exact)
    part_key = over_tokens(proj_key, key_upstream.astype(jnp.float32), exact)
    grad_branch = lax.psum_scatter(
        over_tokens(whole_values, branch_upstream), "fs", scatter_dimension=0, tiled=True
    )
    own_branch = lax.dynamic_slice_in_dim(branch_basis, col_index * features, features, 0).astype(
        jnp.float32
    )
    part_branch = jnp.dot(grad_branch, own_branch, precision=exact)
    query_low, key_low = lax.psum((part_query, part_key), "fs")
    branch_low = lax.psum(part_branch, "tp")
    local_squares = (jnp.sum(query_low * query_low) + jnp.sum(key_low * key_low)) / n_rows
    local_squares = local_squares + jnp.sum(branch_low * branch_low) / n_cols
    total = lax.psum(local_squares, ("fs", "tp"))
    entries = rank * n_cols * (2 * query_local + key_local)
    rms_value = jnp.sqrt(total / float(entries))
    clip = 1.0 / jnp.maximum(1.0, rms_value / CLIP_RMS)
    q_first, q_second, q_dir = moments(query_first, query_second, query_low, clip)
    k_first, k_second, k_dir = moments(key_first, key_second, key_low, clip)
    b_first, b_second, b_dir = moments(branch_first, branch_second, branch_low, clip)
    step_rows_query = lax.dynamic_slice_in_dim(query_basis, row_index * rows_in, rows_in, 0).astype(
        jnp.float32
    )
    step_rows_key = lax.dynamic_slice_in_dim(key_basis, row_index * rows_in, rows_in, 0).astype(
        jnp.float32
    )
    query_step = jnp.dot(step_rows_query, q_dir, precision=exact)
    key_step = jnp.dot(step_rows_key, k_dir, precision=exact)
    branch_step = jnp.dot(b_dir, own_branch.T, precision=exact)
    query_updated = query_master - LEARN * query_step
    key_updated = key_master - LEARN * key_step
    branch_updated = branch_master - LEARN * branch_step
    query_copy, key_copy, branch_copy = (
        lax.all_gather(query_updated.astype(jnp.bfloat16), "fs", axis=0, tiled=True),
        lax.all_gather(key_updated.astype(jnp.bfloat16), "fs", axis=0, tiled=True),
        lax.all_gather(branch_updated.astype(jnp.bfloat16), "fs", axis=0, tiled=True),
    )
    return (
        query_step,
        key_step,
        branch_step,
        query_updated,
        key_updated,
        branch_updated,
        query_copy,
        key_copy,
        branch_copy,
        q_first,
        q_second,
        k_first,
        k_second,
        b_first,
        b_second,
    )


def solution(mesh):
    return jax.shard_map(
        per_device,
        mesh=mesh,
        in_specs=(
            P("fs", "tp"),
            P("fs", "tp"),
            P("fs", "tp"),
            P("fs", "tp"),
            P("fs", "tp"),
            P("fs", "tp"),
            P("fs", "tp"),
            P("fs", "tp"),
            P(),
            P(),
            P(),
            P(None, "tp"),
            P(None, "tp"),
            P(None, "tp"),
            P(None, "tp"),
            P("fs", None),
            P("fs", None),
        ),
        out_specs=(
            P("fs", "tp"),
            P("fs", "tp"),
            P("fs", "tp"),
            P("fs", "tp"),
            P("fs", "tp"),
            P("fs", "tp"),
            P(None, "tp"),
            P(None, "tp"),
            P(None, "tp"),
            P(None, "tp"),
            P(None, "tp"),
            P(None, "tp"),
            P(None, "tp"),
            P("fs", None),
            P("fs", None),
        ),
        check_vma=False,
    )
```

profile of v0, /device:TPU:0, one launch (start us, length us, event | category | flops | bytes accessed | tf_op | source)
XLA Modules:
  0.0 502.3 jit_solution(1356573704103843505)
XLA Ops:
  7.2 0.7 all-gather.5.cloned.1.call-update
  8.0 86.4 %all-gather.5.cloned.1.call-done = bf16[1024,4096]{1,0:T(8,128)(2,1)} async-done(((bf16[1024,512]{1,0:T(8,128)(2,1)}), bf16[1024,4096]{1,0:T(8,128)(2,1)}) %all-gather.5.cloned.1.call-update) | async-done | bytes 8388624 | tf_op jit(solution)/shard_map/all_gather | solution.py:59
  94.4 10.4 %fusion.39 = f32[4096,512]{1,0:T(8,128)} fusion(bf16[1024,4096]{1,0:T(8,128)(2,1)} %all-gather.5.cloned.1.call-done, bf16[1024,512]{1,0:T(8,128)(2,1)S(1)} %copy-done), kind=kOutput, calls=%fused_computation.53 | convolution fusion | flops 4294967296 | bytes 17825792 | tf_op jit(solution)/shard_map/dot_general | solution.py:21
  104.9 0.0 all-reduce.5.cloned.1.call-start
  104.9 1.1 copy-done.2
  106.1 2.2 convolution_bitcast_fusion
  108.2 2.2 convolution_bitcast_fusion.1
  110.4 79.4 %reduce-scatter.2.cloned.1.call-done = f32[1024,512]{1,0:T(8,128)} async-done(((f32[4096,512]{1,0:T(8,128)}), f32[1024,512]{1,0:T(8,128)}) %reduce-scatter.2.cloned.1.call-update) | async-done | bytes 2097168 | tf_op jit(solution)/shard_map/reduce_scatter | solution.py:71
  189.8 3.4 fusion.18
  193.3 0.0 all-reduce.7.cloned.1.call-start
  193.4 62.4 %all-reduce.5.cloned.1.call-done = (f32[1024,128]{0,1:T(8,128)}, f32[1024,128]{0,1:T(8,128)}, f32[1024,128]{1,0:T(8,128)}) async-done(((f32[1024,128]{0,1:T(8,128)}, f32[1024,128]{0,1:T(8,128)}, f32[1024,128]{1,0:T(8,128)}), (f32[1024,128]{0,1:T(8,128)}, f32[1024,128]{0,1:T(8,128)}, f32[1024,128]{1,0:T(8,128)})) %all-reduce.5.cloned.1.call-update) | async-done | bytes 1572880 | tf_op jit(solution)/shard_map/psum | solution.py:62
  255.8 2.5 fusion.37
  258.3 1.0 fusion.38
  259.3 0.0 all-gather.9.cloned.1.call-start
  259.4 0.7 multiply_reduce_fusion
  260.7 41.6 %all-reduce.7.cloned.1.call-done = (f32[128,512]{1,0:T(8,128)}, f32[128,128]{1,0:T(8,128)}) async-done(((f32[128,512]{1,0:T(8,128)}, f32[128,128]{1,0:T(8,128)}), (f32[128,512]{1,0:T(8,128)}, f32[128,128]{1,0:T(8,128)})) %all-reduce.7.cloned.1.call-update) | async-done | bytes 327696 | tf_op jit(solution)/shard_map/psum | solution.py:78
  302.3 1.6 multiply_reduce_fusion.1
  303.9 1.5 multiply_reduce_fusion.2
  306.7 39.3 %psum.47 = f32[]{:T(128)} all-reduce(f32[]{:T(128)S(6)} %add.68), channel_id=1, replica_groups=mesh['fs'=4,'tp'=8] {'fs','tp'}, use_global_device_ids=true, to_apply=%region_9.0 | all-reduce | flops 1 | bytes 8 | tf_op jit(solution)/shard_map/psum | solution.py:82
  346.8 0.9 fusion.20
  347.7 2.6 fusion.35
  350.3 1.4 fusion
  351.7 4.7 fusion.34
  356.5 1.2 fusion.5
  357.7 0.4 copy-done.8
  358.1 4.5 fusion.36
  362.7 15.2 %all-gather.9.cloned.1.call-done = bf16[4096,128]{1,0:T(8,128)(2,1)} async-done(((bf16[1024,128]{1,0:T(8,128)(2,1)}), bf16[4096,128]{1,0:T(8,128)(2,1)}) %all-gather.9.cloned.1.call-update) | async-done | bytes 1048592 | tf_op jit(solution)/shard_map/all_gather | solution.py:103
  377.9 54.9 %all-gather.11.cloned.1.call-done = bf16[4096,512]{1,0:T(8,128)(2,1)} async-done(((bf16[1024,512]{1,0:T(8,128)(2,1)}), bf16[4096,512]{1,0:T(8,128)(2,1)}) %all-gather.11.cloned.1.call-update) | async-done | bytes 4194320 | tf_op jit(solution)/shard_map/all_gather | solution.py:104
  432.8 55.0 %all-gather.7.cloned.1.call-done = bf16[4096,512]{1,0:T(8,128)(2,1)} async-done(((bf16[1024,512]{1,0:T(8,128)(2,1)}), bf16[4096,512]{1,0:T(8,128)(2,1)}) %all-gather.7.cloned.1.call-update) | async-done | bytes 4194320 | tf_op jit(solution)/shard_map/all_gather | solution.py:102
  487.8 4.6 copy.40
  492.5 1.0 copy.41
  493.4 2.0 copy.42
  (52 shorter events, 0.4 us)
Async XLA Ops:
  7.2 87.2 %copy-start = (bf16[1024,512]{1,0:T(8,128)(2,1)S(1)}, bf16[1024,512]{1,0:T(8,128)(2,1)}, u32[]{:S(2)}) copy-start(bf16[1024,512]{1,0:T(8,128)(2,1)} %param.21) | copy-start | bytes 3145732
  7.2 87.2 %all-gather.5.cloned.1.call-start = ((), (), s32[]{:S(2)}) async-start(), calls=%async_computation.1 | async-start | bytes 9437184 | tf_op jit(solution)/shard_map/all_gather | solution.py:59
  7.9 181.9 %reduce-scatter.2.cloned.1.call-start = ((), (), s32[]{:S(2)}) async-start(), calls=%async_computation.2 | async-start | bytes 10485760 | tf_op jit(solution)/shard_map/reduce_scatter | solution.py:71
  104.9 1.2 copy-start.2
  104.9 150.9 %all-reduce.5.cloned.1.call-start = ((), (), s32[]{:S(2)}) async-start(), calls=%async_computation.6 | async-start | bytes 3145728 | tf_op jit(solution)/shard_map/psum | solution.py:62
  110.4 145.4 %copy-start.11 = (bf16[1024,512]{1,0:T(8,128)(2,1)S(1)}, bf16[1024,512]{1,0:T(8,128)(2,1)}, u32[]{:S(2)}) copy-start(bf16[1024,512]{1,0:T(8,128)(2,1)} %param.18) | copy-start | bytes 3145732
  193.3 65.0 %copy-start.19 = (bf16[1024,128]{1,0:T(8,128)(2,1)S(1)}, bf16[1024,128]{1,0:T(8,128)(2,1)}, u32[]{:S(2)}) copy-start(bf16[1024,128]{1,0:T(8,128)(2,1)} %param.19) | copy-start | bytes 786436
  193.3 153.5 %copy-start.20 = (f32[128,128]{1,0:T(8,128)S(1)}, f32[128,128]{1,0:T(8,128)}, u32[]{:S(2)}) copy-start(f32[128,128]{1,0:T(8,128)} %param.31) | copy-start | bytes 196612
  193.3 153.5 %copy-start.21 = (f32[128,128]{1,0:T(8,128)S(1)}, f32[128,128]{1,0:T(8,128)}, u32[]{:S(2)}) copy-start(f32[128,128]{1,0:T(8,128)} %param.30) | copy-start | bytes 196612
  193.3 109.0 %all-reduce.7.cloned.1.call-start = ((), (), s32[]{:S(2)}) async-start(), calls=%async_computation.7 | async-start | bytes 655360 | tf_op jit(solution)/shard_map/psum | solution.py:78
  255.8 2.5 copy-start.15
  255.8 3.6 copy-start.6
  255.8 91.9 %copy-start.14 = (f32[1024,128]{1,0:T(8,128)S(1)}, f32[1024,128]{1,0:T(8,128)}, u32[]{:S(2)}) copy-start(f32[1024,128]{1,0:T(8,128)} %param.23) | copy-start | bytes 1572868
  259.3 118.6 %all-gather.9.cloned.1.call-start = ((), (), s32[]{:S(2)}) async-start(), calls=%async_computation.4 | async-start | bytes 1310720 | tf_op jit(solution)/shard_map/all_gather | solution.py:103
  347.6 4.0 copy-start.17
  347.6 4.0 copy-start.18
  347.7 4.0 copy-start.7
  350.3 82.5 %all-gather.11.cloned.1.call-start = ((), (), s32[]{:S(2)}) async-start(), calls=%async_computation.5 | async-start | bytes 5242880 | tf_op jit(solution)/shard_map/all_gather | solution.py:104
  351.7 4.7 copy-start.4
  351.7 4.7 copy-start.5
  351.7 4.8 copy-start.12
  351.7 4.8 copy-start.16
  356.4 1.7 copy-start.8
  356.4 131.4 %all-gather.7.cloned.1.call-start = ((), (), s32[]{:S(2)}) async-start(), calls=%async_computation.3 | async-start | bytes 5242880 | tf_op jit(solution)/shard_map/all_gather | solution.py:102
  357.7 5.0 copy-start.9
  357.7 5.0 copy-start.10
  487.8 4.6 copy-start.13
  487.8 5.6 %copy-start.3 = (bf16[4096,512]{1,0:T(8,128)(2,1)S(1)}, bf16[4096,512]{1,0:T(8,128)(2,1)}, u32[]{:S(2)}) copy-start(bf16[4096,512]{1,0:T(8,128)(2,1)} %all-gather.11.cloned.1.call-done) | copy-start | bytes 12582916
  493.4 2.0 copy-start.1
Sparse Core Ops, SparseCore 0:
  9.6 84.7 all-gather.4
  105.0 84.7 reduce-scatter.1
  193.6 62.1 all-reduce.4
  259.4 42.8 all-reduce.6
  350.4 27.4 all-gather.8
  380.2 52.5 all-gather.10
  435.2 52.5 all-gather.6
where the time goes:
time: 503 us; the launch traced here: 502 us
  waiting for transfers between devices  396 us (79%)
  blocking collectives  39.3 us (8%)
  matrix products  33.4 us (7%)
  between operations  17 us (3%)
  local copies, waits for them, and re-layouts  9.28 us (2%)
  other arithmetic  7.2 us (1%)
    all_gather x1, waiting for transfers between devices, per_device(): whole_values = lax.all_gather(head_outputs, 'tp', axis=1, tiled=True)  86.4 us
    reduce_scatter x1, waiting for transfers between devices, per_device(): lax.psum_scatter(over_tokens(whole_values, branch_upstream), 'fs', scatte...  79.4 us
    psum x1, waiting for transfers between devices, per_device(): lax.psum((jnp.dot(normed_inputs, block_query, preferred_element_type=jnp....  62.4 us
    all_gather x1, waiting for transfers between devices, per_device(): lax.all_gather(query_updated.astype(jnp.bfloat16), 'fs', axis=0, tiled=True)  55 us
    all_gather x1, waiting for transfers between devices, per_device(): lax.all_gather(branch_updated.astype(jnp.bfloat16), 'fs', axis=0, tiled=T...  54.9 us
    psum x1, waiting for transfers between devices, per_device(): query_low, key_low = lax.psum((part_query, part_key), 'fs')  41.6 us
    psum x1, blocking collectives, per_device(): total = lax.psum(local_squares, ('fs', 'tp'))  39.3 us
    all_gather x1, waiting for transfers between devices, per_device(): lax.all_gather(key_updated.astype(jnp.bfloat16), 'fs', axis=0, tiled=True)  15.2 us
  transfers between devices with their start and end apart: 7, of which 7 were waited for; matrix products, arithmetic and copies ran while one was open for 3% of the time, Pallas kernels for 0%

commit v1 on v0

--- a/solution.py
+++ b/solution.py
@@ -56,7 +56,12 @@
     key_local = key_upstream.shape[1]
     rows_in = query_master.shape[0]
     rank = query_basis.shape[1]
-    whole_values = lax.all_gather(head_outputs, "tp", axis=1, tiled=True)
+    ring = [head_outputs]
+    for hop in range(7):
+        ring.append(lax.ppermute(ring[-1], "tp", [(dev, (dev + 1) % 8) for dev in range(8)]))
+    whole_values = jnp.roll(
+        jnp.concatenate(ring[::-1], axis=1), (lax.axis_index("tp") + 1) * ring[0].shape[1], axis=1
+    )
     block_query = lax.dynamic_slice_in_dim(query_basis, col_index * features, features, 0)
     block_key = lax.dynamic_slice_in_dim(key_basis, col_index * features, features, 0)
     proj_query, proj_key = lax.psum(

time: 503 us -> 548 us (1.089)
  waiting for transfers between devices: 396 us -> 421 us
  local copies, waits for them, and re-layouts: 9.28 us -> 28.2 us
    ppermute x0 -> x7, waiting for transfers between devices: none -> 113 us  [per_device(): lax.ppermute(ring[-1], 'tp', [(dev, (dev + 1) % 8) for dev in range(8)])]
    all_gather x1 -> x0, waiting for transfers between devices: 86.4 us -> none  [per_device(): whole_values = lax.all_gather(head_outputs, 'tp', axis=1, tiled=True)]
    unnamed x47 -> x68, local copies, waits for them, and re-layouts: 9.28 us -> 28.1 us
  transfers between devices with their start and end apart: 7 -> 13, of which waited for: 7 -> 13; matrix products, arithmetic and copies ran while one was open for 3% -> 4% of each run, Pallas kernels for 0% -> 0%
where the time goes in v1:
time: 548 us; the launch traced here: 547 us
  waiting for transfers between devices  421 us (77%)
  blocking collectives  39.3 us (7%)
  matrix products  32.8 us (6%)
  local copies, waits for them, and re-layouts  28.2 us (5%)
  between operations  17.2 us (3%)
  other arithmetic  8.13 us (1%)
    ppermute x7, waiting for transfers between devices, per_device(): lax.ppermute(ring[-1], 'tp', [(dev, (dev + 1) % 8) for dev in range(8)])  113 us
    reduce_scatter x1, waiting for transfers between devices, per_device(): lax.psum_scatter(over_tokens(whole_values, branch_upstream), 'fs', scatte...  80.7 us
    psum x1, waiting for transfers between devices, per_device(): lax.psum((jnp.dot(normed_inputs, block_query, preferred_element_type=jnp....  62.5 us
    all_gather x1, waiting for transfers between devices, per_device(): lax.all_gather(query_updated.astype(jnp.bfloat16), 'fs', axis=0, tiled=True)  54.9 us
    all_gather x1, waiting for transfers between devices, per_device(): lax.all_gather(branch_updated.astype(jnp.bfloat16), 'fs', axis=0, tiled=T...  54.9 us
    psum x1, waiting for transfers between devices, per_device(): query_low, key_low = lax.psum((part_query, part_key), 'fs')  40.5 us
    psum x1, blocking collectives, per_device(): total = lax.psum(local_squares, ('fs', 'tp'))  39.3 us
    unnamed x68, local copies, waits for them, and re-layouts  28.1 us
  transfers between devices with their start and end apart: 13, of which 13 were waited for; matrix products, arithmetic and copies ran while one was open for 4% of the time, Pallas kernels for 0%

profile of v1, /device:TPU:0, one launch (start us, length us, event | category | flops | bytes accessed | tf_op | source)
XLA Modules:
  0.0 547.2 jit_solution(6530817916398425807)
XLA Ops:
  7.8 16.7 %collective-permute-done = bf16[1024,512]{1,0:T(8,128)(2,1)S(1)} collective-permute-done((bf16[1024,512]{1,0:T(8,128)(2,1)}, bf16[1024,512]{1,0:T(8,128)(2,1)S(1)}, u32[]{:S(2)}, u32[]{:S(2)}) %collective-permute-start) | collective-permute-done | bytes 1048608 | tf_op jit(solution)/shard_map/ppermute | solution.py:61
  24.5 16.0 %collective-permute-done.1 = bf16[1024,512]{1,0:T(8,128)(2,1)S(1)} collective-permute-done((bf16[1024,512]{1,0:T(8,128)(2,1)S(1)}, bf16[1024,512]{1,0:T(8,128)(2,1)S(1)}, u32[]{:S(2)}, u32[]{:S(2)}) %collective-permute-start.1) | collective-permute-done | bytes 1048608 | tf_op jit(solution)/shard_map/ppermute | solution.py:61
  41.5 16.0 %collective-permute-done.2 = bf16[1024,512]{1,0:T(8,128)(2,1)S(1)} collective-permute-done((bf16[1024,512]{1,0:T(8,128)(2,1)S(1)}, bf16[1024,512]{1,0:T(8,128)(2,1)S(1)}, u32[]{:S(2)}, u32[]{:S(2)}) %collective-permute-start.2) | collective-permute-done | bytes 1048608 | tf_op jit(solution)/shard_map/ppermute | solution.py:61
  58.5 16.0 %collective-permute-done.3 = bf16[1024,512]{1,0:T(8,128)(2,1)S(1)} collective-permute-done((bf16[1024,512]{1,0:T(8,128)(2,1)S(1)}, bf16[1024,512]{1,0:T(8,128)(2,1)S(1)}, u32[]{:S(2)}, u32[]{:S(2)}) %collective-permute-start.3) | collective-permute-done | bytes 1048608 | tf_op jit(solution)/shard_map/ppermute | solution.py:61
  75.5 16.0 %collective-permute-done.4 = bf16[1024,512]{1,0:T(8,128)(2,1)S(1)} collective-permute-done((bf16[1024,512]{1,0:T(8,128)(2,1)S(1)}, bf16[1024,512]{1,0:T(8,128)(2,1)S(1)}, u32[]{:S(2)}, u32[]{:S(2)}) %collective-permute-start.4) | collective-permute-done | bytes 1048608 | tf_op jit(solution)/shard_map/ppermute | solution.py:61
  92.5 16.1 %collective-permute-done.5 = bf16[1024,512]{1,0:T(8,128)(2,1)} collective-permute-done((bf16[1024,512]{1,0:T(8,128)(2,1)S(1)}, bf16[1024,512]{1,0:T(8,128)(2,1)}, u32[]{:S(2)}, u32[]{:S(2)}) %collective-permute-start.5) | collective-permute-done | bytes 1048608 | tf_op jit(solution)/shard_map/ppermute | solution.py:61
  108.6 16.3 %collective-permute-done.6 = bf16[1024,512]{1,0:T(8,128)(2,1)} collective-permute-done((bf16[1024,512]{1,0:T(8,128)(2,1)}, bf16[1024,512]{1,0:T(8,128)(2,1)}, u32[]{:S(2)}, u32[]{:S(2)}) %collective-permute-start.6) | collective-permute-done | bytes 1048608 | tf_op jit(solution)/shard_map/ppermute | solution.py:61
  126.3 1.3 constant_dynamic-update-slice_fusion.14
  130.4 1.3 constant_dynamic-update-slice_fusion.11
  138.2 7.0 %fusion = f32[4096,512]{1,0:T(8,128)} fusion(bf16[1024,512]{1,0:T(8,128)(2,1)S(1)} %copy-done, bf16[1024,8192]{1,0:T(8,128)(2,1)S(1)} %constant_dynamic-update-slice_fusion, s32[]{:T(128)S(6)} %select_n.25), kind=kOutput, calls=%fused_computation | convolution fusion | flops 4294967296 | bytes 17825796 | tf_op jit(solution)/shard_map/dot_general | solution.py:21
  145.3 2.3 convolution_bitcast_fusion
  147.6 2.2 convolution_bitcast_fusion.1
  149.7 80.7 %reduce-scatter.2.cloned.1.call-done = f32[1024,512]{1,0:T(8,128)} async-done(((f32[4096,512]{1,0:T(8,128)}), f32[1024,512]{1,0:T(8,128)}) %reduce-scatter.2.cloned.1.call-update) | async-done | bytes 2097168 | tf_op jit(solution)/shard_map/reduce_scatter | solution.py:76
  230.4 3.4 fusion.20
  233.9 62.5 %all-reduce.5.cloned.1.call-done = (f32[1024,128]{0,1:T(8,128)}, f32[1024,128]{0,1:T(8,128)}, f32[1024,128]{1,0:T(8,128)}) async-done(((f32[1024,128]{0,1:T(8,128)}, f32[1024,128]{0,1:T(8,128)}, f32[1024,128]{1,0:T(8,128)}), (f32[1024,128]{0,1:T(8,128)}, f32[1024,128]{0,1:T(8,128)}, f32[1024,128]{1,0:T(8,128)})) %all-reduce.5.cloned.1.call-update) | async-done | bytes 1572880 | tf_op jit(solution)/shard_map/psum | solution.py:67
  296.4 2.3 fusion.40
  298.8 2.2 fusion.41
  301.0 1.8 multiply_reduce_fusion
  303.4 40.5 %all-reduce.7.cloned.1.call-done = (f32[128,512]{1,0:T(8,128)}, f32[128,128]{1,0:T(8,128)}) async-done(((f32[128,512]{1,0:T(8,128)}, f32[128,128]{1,0:T(8,128)}), (f32[128,512]{1,0:T(8,128)}, f32[128,128]{1,0:T(8,128)})) %all-reduce.7.cloned.1.call-update) | async-done | bytes 327696 | tf_op jit(solution)/shard_map/psum | solution.py:83
  344.0 1.6 multiply_reduce_fusion.1
  345.6 1.5 multiply_reduce_fusion.2
  348.3 39.3 %psum.47 = f32[]{:T(128)} all-reduce(f32[]{:T(128)S(6)} %add.84), channel_id=1, replica_groups=mesh['fs'=4,'tp'=8] {'fs','tp'}, use_global_device_ids=true, to_apply=%region_9.10 | all-reduce | flops 1 | bytes 8 | tf_op jit(solution)/shard_map/psum | solution.py:87
  389.3 2.4 fusion.38
  391.8 1.4 fusion.2
  393.2 5.5 %fusion.37 = (bf16[1024,512]{1,0:T(8,128)(2,1)}, f32[1024,512]{1,0:T(8,128)}, f32[1024,512]{1,0:T(8,128)}) fusion(f32[1024,512]{1,0:T(8,128)} %param.24, bf16[4096,128]{1,0:T(8,128)(2,1)} %param.27, s32[]{:T(128)S(6)} %select_n.23, f32[1024,128]{1,0:T(8,128)S(1)} %get-tuple-element.63, f32[1024,128]{1,0:T(8,128)S(1)} %get-tuple-element.64), kind=kOutput, calls=%fused_computation.67 | convolution fusion | flops 807141376 | bytes 8519684 | tf_op jit(solution)/shard_map/dot_general | solution.py:102
  399.9 5.5 %fusion.39 = (bf16[1024,512]{1,0:T(8,128)(2,1)}, f32[1024,512]{1,0:T(8,128)}, f32[1024,512]{1,0:T(8,128)}) fusion(f32[1024,512]{1,0:T(8,128)} %param.22, f32[128,512]{1,0:T(8,128)S(1)} %get-tuple-element.59, f32[128,512]{1,0:T(8,128)S(1)} %get-tuple-element.60, bf16[4096,128]{1,0:T(8,128)(2,1)} %param.25, s32[]{:T(128)S(6)} %select_n.22), kind=kOutput, calls=%fused_computation.69 | convolution fusion | flops 807010304 | bytes 8126468 | tf_op jit(solution)/shard_map/dot_general | solution.py:100
  405.4 13.9 %all-gather.6.cloned.1.call-done = bf16[4096,128]{1,0:T(8,128)(2,1)} async-done(((bf16[1024,128]{1,0:T(8,128)(2,1)}), bf16[4096,128]{1,0:T(8,128)(2,1)}) %all-gather.6.cloned.1.call-update) | async-done | bytes 1048592 | tf_op jit(solution)/shard_map/all_gather | solution.py:108
  419.4 54.9 %all-gather.8.cloned.1.call-done = bf16[4096,512]{1,0:T(8,128)(2,1)} async-done(((bf16[1024,512]{1,0:T(8,128)(2,1)}), bf16[4096,512]{1,0:T(8,128)(2,1)}) %all-gather.8.cloned.1.call-update) | async-done | bytes 4194320 | tf_op jit(solution)/shard_map/all_gather | solution.py:109
  474.2 54.9 %all-gather.4.cloned.1.call-done = bf16[4096,512]{1,0:T(8,128)(2,1)} async-done(((bf16[1024,512]{1,0:T(8,128)(2,1)}), bf16[4096,512]{1,0:T(8,128)(2,1)}) %all-gather.4.cloned.1.call-update) | async-done | bytes 4194320 | tf_op jit(solution)/shard_map/all_gather | solution.py:107
  529.1 4.5 copy.55
  533.6 2.3 copy.56
  535.8 4.5 copy.57
  (85 shorter events, 17.1 us)
Async XLA Ops:
  7.2 130.9 %copy-start = (bf16[1024,512]{1,0:T(8,128)(2,1)S(1)}, bf16[1024,512]{1,0:T(8,128)(2,1)}, u32[]{:S(2)}) copy-start(bf16[1024,512]{1,0:T(8,128)(2,1)} %param.21) | copy-start | bytes 3145732
  7.2 130.8 %copy-start.3 = (bf16[1024,512]{1,0:T(8,128)(2,1)S(1)}, bf16[1024,512]{1,0:T(8,128)(2,1)}, u32[]{:S(2)}) copy-start(bf16[1024,512]{1,0:T(8,128)(2,1)} %param.20) | copy-start | bytes 3145732
  7.2 223.2 %reduce-scatter.2.cloned.1.call-start = ((), (), s32[]{:S(2)}) async-start(), calls=%async_computation.1 | async-start | bytes 10485760 | tf_op jit(solution)/shard_map/reduce_scatter | solution.py:76
  7.3 17.3 %collective-permute-start = (bf16[1024,512]{1,0:T(8,128)(2,1)}, bf16[1024,512]{1,0:T(8,128)(2,1)S(1)}, u32[]{:S(2)}, u32[]{:S(2)}) collective-permute-start(bf16[1024,512]{1,0:T(8,128)(2,1)} %param.20), channel_id=1, source_target_pairs={{0,1},{1,2},{2,3},{3,4},{4,5},{5,6},{6,7},{7,0},{8,9},{9,10},{10,1... | collective-permute-start | bytes 3145736 | tf_op jit(solution)/shard_map/ppermute | solution.py:61
  24.5 16.0 %collective-permute-start.1 = (bf16[1024,512]{1,0:T(8,128)(2,1)S(1)}, bf16[1024,512]{1,0:T(8,128)(2,1)S(1)}, u32[]{:S(2)}, u32[]{:S(2)}) collective-permute-start(bf16[1024,512]{1,0:T(8,128)(2,1)S(1)} %collective-permute-done), channel_id=1, source_target_pairs={{0,1},{1,2},{2,3},{3,4},{4,5},{5,6},{6,7},{7,0},{8,9},{9,10},{10,1... | collective-permute-start | bytes 3145736 | tf_op jit(solution)/shard_map/ppermute | solution.py:61
  41.5 16.0 %collective-permute-start.2 = (bf16[1024,512]{1,0:T(8,128)(2,1)S(1)}, bf16[1024,512]{1,0:T(8,128)(2,1)S(1)}, u32[]{:S(2)}, u32[]{:S(2)}) collective-permute-start(bf16[1024,512]{1,0:T(8,128)(2,1)S(1)} %collective-permute-done.1), channel_id=1, source_target_pairs={{0,1},{1,2},{2,3},{3,4},{4,5},{5,6},{6,7},{7,0},{8,9},{9,10},{10,1... | collective-permute-start | bytes 3145736 | tf_op jit(solution)/shard_map/ppermute | solution.py:61
  58.5 16.0 %collective-permute-start.3 = (bf16[1024,512]{1,0:T(8,128)(2,1)S(1)}, bf16[1024,512]{1,0:T(8,128)(2,1)S(1)}, u32[]{:S(2)}, u32[]{:S(2)}) collective-permute-start(bf16[1024,512]{1,0:T(8,128)(2,1)S(1)} %collective-permute-done.2), channel_id=1, source_target_pairs={{0,1},{1,2},{2,3},{3,4},{4,5},{5,6},{6,7},{7,0},{8,9},{9,10},{10,1... | collective-permute-start | bytes 3145736 | tf_op jit(solution)/shard_map/ppermute | solution.py:61
  75.5 16.0 %collective-permute-start.4 = (bf16[1024,512]{1,0:T(8,128)(2,1)S(1)}, bf16[1024,512]{1,0:T(8,128)(2,1)S(1)}, u32[]{:S(2)}, u32[]{:S(2)}) collective-permute-start(bf16[1024,512]{1,0:T(8,128)(2,1)S(1)} %collective-permute-done.3), channel_id=1, source_target_pairs={{0,1},{1,2},{2,3},{3,4},{4,5},{5,6},{6,7},{7,0},{8,9},{9,10},{10,1... | collective-permute-start | bytes 3145736 | tf_op jit(solution)/shard_map/ppermute | solution.py:61
  92.5 16.1 %collective-permute-start.5 = (bf16[1024,512]{1,0:T(8,128)(2,1)S(1)}, bf16[1024,512]{1,0:T(8,128)(2,1)}, u32[]{:S(2)}, u32[]{:S(2)}) collective-permute-start(bf16[1024,512]{1,0:T(8,128)(2,1)S(1)} %collective-permute-done.4), channel_id=1, source_target_pairs={{0,1},{1,2},{2,3},{3,4},{4,5},{5,6},{6,7},{7,0},{8,9},{9,10},{10,1... | collective-permute-start | bytes 3145736 | tf_op jit(solution)/shard_map/ppermute | solution.py:61
  108.6 16.3 %collective-permute-start.6 = (bf16[1024,512]{1,0:T(8,128)(2,1)}, bf16[1024,512]{1,0:T(8,128)(2,1)}, u32[]{:S(2)}, u32[]{:S(2)}) collective-permute-start(bf16[1024,512]{1,0:T(8,128)(2,1)} %collective-permute-done.5), channel_id=1, source_target_pairs={{0,1},{1,2},{2,3},{3,4},{4,5},{5,6},{6,7},{7,0},{8,9},{9,10},{10,1... | collective-permute-start | bytes 3145736 | tf_op jit(solution)/shard_map/ppermute | solution.py:61
  108.6 28.8 %copy-start.9 = (bf16[1024,512]{1,0:T(8,128)(2,1)S(1)}, bf16[1024,512]{1,0:T(8,128)(2,1)}, u32[]{:S(2)}) copy-start(bf16[1024,512]{1,0:T(8,128)(2,1)} %copy-done.8) | copy-start | bytes 3145732
  108.6 29.0 %copy-start.7 = (bf16[1024,512]{1,0:T(8,128)(2,1)S(1)}, bf16[1024,512]{1,0:T(8,128)(2,1)}, u32[]{:S(2)}) copy-start(bf16[1024,512]{1,0:T(8,128)(2,1)} %copy-done.6) | copy-start | bytes 3145732
  108.6 29.1 %copy-start.5 = (bf16[1024,512]{1,0:T(8,128)(2,1)S(1)}, bf16[1024,512]{1,0:T(8,128)(2,1)}, u32[]{:S(2)}) copy-start(bf16[1024,512]{1,0:T(8,128)(2,1)} %copy-done.4) | copy-start | bytes 3145732
  138.1 158.3 %copy-start.16 = (bf16[1024,512]{1,0:T(8,128)(2,1)S(1)}, bf16[1024,512]{1,0:T(8,128)(2,1)}, u32[]{:S(2)}) copy-start(bf16[1024,512]{1,0:T(8,128)(2,1)} %param.18) | copy-start | bytes 3145732
  145.2 243.2 %copy-start.23 = (f32[128,128]{1,0:T(8,128)S(1)}, f32[128,128]{1,0:T(8,128)}, u32[]{:S(2)}) copy-start(f32[128,128]{1,0:T(8,128)} %param.31) | copy-start | bytes 196612
  145.2 243.2 %copy-start.24 = (f32[128,128]{1,0:T(8,128)S(1)}, f32[128,128]{1,0:T(8,128)}, u32[]{:S(2)}) copy-start(f32[128,128]{1,0:T(8,128)} %param.30) | copy-start | bytes 196612
  145.2 244.1 %copy-start.17 = (f32[1024,128]{1,0:T(8,128)S(1)}, f32[1024,128]{1,0:T(8,128)}, u32[]{:S(2)}) copy-start(f32[1024,128]{1,0:T(8,128)} %param.23) | copy-start | bytes 1572868
  145.2 246.6 %copy-start.18 = (f32[1024,128]{1,0:T(8,128)S(1)}, f32[1024,128]{1,0:T(8,128)}, u32[]{:S(2)}) copy-start(f32[1024,128]{1,0:T(8,128)} %param.33) | copy-start | bytes 1572868
  145.2 253.6 %copy-start.19 = (f32[128,512]{1,0:T(8,128)S(1)}, f32[128,512]{1,0:T(8,128)}, u32[]{:S(2)}) copy-start(f32[128,512]{1,0:T(8,128)} %param.29) | copy-start | bytes 786436
  145.2 151.2 %all-reduce.5.cloned.1.call-start = ((), (), s32[]{:S(2)}) async-start(), calls=%async_computation.5 | async-start | bytes 3145728 | tf_op jit(solution)/shard_map/psum | solution.py:67
  233.9 110.1 %all-reduce.7.cloned.1.call-start = ((), (), s32[]{:S(2)}) async-start(), calls=%async_computation.6 | async-start | bytes 655360 | tf_op jit(solution)/shard_map/psum | solution.py:83
  298.8 100.0 %copy-start.20 = (f32[128,512]{1,0:T(8,128)S(1)}, f32[128,512]{1,0:T(8,128)}, u32[]{:S(2)}) copy-start(f32[128,512]{1,0:T(8,128)} %param.28) | copy-start | bytes 786436
  300.9 118.4 %all-gather.6.cloned.1.call-start = ((), (), s32[]{:S(2)}) async-start(), calls=%async_computation.3 | async-start | bytes 1310720 | tf_op jit(solution)/shard_map/all_gather | solution.py:108
  389.3 144.3 %copy-start.21 = (f32[128,128]{1,0:T(8,128)}, f32[128,128]{1,0:T(8,128)S(1)}, u32[]{:S(2)}) copy-start(f32[128,128]{1,0:T(8,128)S(1)} %get-tuple-element.62) | copy-start | bytes 196612
  389.3 144.3 %copy-start.22 = (f32[128,128]{1,0:T(8,128)}, f32[128,128]{1,0:T(8,128)S(1)}, u32[]{:S(2)}) copy-start(f32[128,128]{1,0:T(8,128)S(1)} %get-tuple-element.61) | copy-start | bytes 196612
  391.7 82.5 %all-gather.8.cloned.1.call-start = ((), (), s32[]{:S(2)}) async-start(), calls=%async_computation.4 | async-start | bytes 5242880 | tf_op jit(solution)/shard_map/all_gather | solution.py:109
  393.2 147.2 %copy-start.12 = (f32[1024,128]{1,0:T(8,128)}, f32[1024,128]{1,0:T(8,128)S(1)}, u32[]{:S(2)}) copy-start(f32[1024,128]{1,0:T(8,128)S(1)} %get-tuple-element.64) | copy-start | bytes 1572868
  393.2 147.1 %copy-start.13 = (f32[1024,128]{1,0:T(8,128)}, f32[1024,128]{1,0:T(8,128)S(1)}, u32[]{:S(2)}) copy-start(f32[1024,128]{1,0:T(8,128)S(1)} %get-tuple-element.63) | copy-start | bytes 1572868
  393.2 147.1 %copy-start.1 = (bf16[1024,512]{1,0:T(8,128)(2,1)S(1)}, bf16[1024,512]{1,0:T(8,128)(2,1)}, u32[]{:S(2)}) copy-start(bf16[1024,512]{1,0:T(8,128)(2,1)} %param.21) | copy-start | bytes 3145732
  398.7 130.4 %all-gather.4.cloned.1.call-start = ((), (), s32[]{:S(2)}) async-start(), calls=%async_computation.2 | async-start | bytes 5242880 | tf_op jit(solution)/shard_map/all_gather | solution.py:107
  399.9 140.5 %copy-start.14 = (f32[128,512]{1,0:T(8,128)}, f32[128,512]{1,0:T(8,128)S(1)}, u32[]{:S(2)}) copy-start(f32[128,512]{1,0:T(8,128)S(1)} %get-tuple-element.60) | copy-start | bytes 786436
  399.9 140.4 %copy-start.15 = (f32[128,512]{1,0:T(8,128)}, f32[128,512]{1,0:T(8,128)S(1)}, u32[]{:S(2)}) copy-start(f32[128,512]{1,0:T(8,128)S(1)} %get-tuple-element.59) | copy-start | bytes 786436
  (6 other events, 39.7 us)
Sparse Core Ops, SparseCore 0:
  145.3 85.0 reduce-scatter.1
  234.2 62.2 all-reduce.4
  301.1 42.8 all-reduce.6
  391.9 27.4 all-gather.5
  421.6 52.5 all-gather.7
  476.5 52.5 all-gather.3
